TPU v7x, 128 devices: a whole 4x4x4 slice. The times are simulated.
128 devices in a mesh: sp: 32 (over z, y, core), tp: 4 (over x).
Axes of the slice: x: 4, y: 4, z: 4, core: 2. Of those that a mesh axis runs over, the one named last changes fastest.
Arguments:
- residual: bfloat16 [32768, 2048], P('sp'), may hold values from -8 to 8
- query_wide: bfloat16 [32768, 1024], P('sp', 'tp'), may hold values from -6 to 6
- key_wide: bfloat16 [32768, 1024], P('sp', 'tp'), may hold values from -6 to 6
- value_wide: bfloat16 [32768, 2048], P('sp', 'tp'), may hold values from -6 to 6
- decay_wide: bfloat16 [32768, 1024], P('sp', 'tp'), may hold values from -12 to 12
- gate_wide: bfloat16 [32768, 2048], P('sp', 'tp'), may hold values from -6 to 6
- query_narrow: bfloat16 [32768, 512], P('sp', 'tp'), may hold values from -6 to 6
- key_narrow: bfloat16 [32768, 512], P('sp', 'tp'), may hold values from -6 to 6
- value_narrow: bfloat16 [32768, 2048], P('sp', 'tp'), may hold values from -6 to 6
- decay_narrow: bfloat16 [32768, 512], P('sp', 'tp'), may hold values from -12 to 12
- gate_narrow: bfloat16 [32768, 2048], P('sp', 'tp'), may hold values from -6 to 6
- head_gain: float32 [512], replicated, may hold values from 0.1 to 1.9
- out_wide: bfloat16 [2048, 2048], P('tp'), may hold values from -0.125 to 0.125
- out_narrow: bfloat16 [2048, 2048], P('tp'), may hold values from -0.125 to 0.125
- mlp_gain: float32 [2048], replicated, may hold values from 0.1 to 1.9
- up_weight: bfloat16 [2048, 4096], P('sp', 'tp'), may hold values from -0.125 to 0.125
- down_weight: bfloat16 [4096, 2048], P('tp', 'sp'), may hold values from -0.09375 to 0.09375
Outputs:
- layer_out: bfloat16 [32768, 2048], P('sp', 'tp')
All inputs are finite; a program needn't handle non-finite values.
Results may differ from a plain program's by a relative error of at most 0.017.
Values may be sent and summed in bfloat16 or wider, within the bound.
A program may use at most 128 MiB of HBM per device.

v0:
```python
import jax
import jax.numpy as jnp
from jax import lax
from jax.sharding import PartitionSpec as P

HEADS = 4
BLOCK = 64
EPS = 1e-05
DECAY_NORMALIZER = 16.0
HIGHEST = lax.Precision.HIGHEST


def turned_gather(arrays, axis, dims):
    turned = [jnp.moveaxis(a, dim, 0) for a, dim in zip(arrays, dims)]
    both = jnp.concatenate([t.reshape(len(t), -1) for t in turned], axis=1)
    whole, at, finished = (lax.all_gather(both, axis, axis=0, tiled=True), 0, [])
    for t, dim in zip(turned, dims):
        section = whole[:, at : at + t[0].size].reshape(-1, *t.shape[1:])
        finished.append(jnp.moveaxis(section, 0, dim))
        at += t[0].size
    return tuple(finished)


def entering(array, axis, join, neutral):
    place = lax.axis_index(axis)
    gathered = jax.tree.map(
        lambda a, kind: lax.all_gather(a.astype(kind), axis),
        array,
        (jnp.bfloat16, jnp.bfloat16, jnp.bfloat16, jnp.bfloat16),
    )
    state = jax.tree.map(lambda a, e: jnp.zeros_like(a) + jnp.asarray(e, a.dtype), array, neutral)

    def one(step, state):
        return join(
            state,
            jax.tree.map(
                lambda a, own: lax.dynamic_index_in_dim(a, step, 0, False).astype(own.dtype),
                gathered,
                array,
            ),
        )

    return lax.fori_loop(0, place, one, state)


def split_up(array, dim, count):
    dims = array.shape
    pieces = array.reshape(*dims[:dim], count, dims[dim] // count, *dims[dim + 1 :])
    return jnp.moveaxis(pieces, dim, 0)


def sum_at_owner(array, axis, dim):
    count = lax.axis_size(axis)
    pieces = lax.all_to_all(split_up(array, dim, count), axis, 0, 0, tiled=True)
    return jnp.sum(pieces.astype(jnp.float32), axis=0)


def sent_to_all(array, axis):
    copies = jnp.broadcast_to(array, (lax.axis_size(axis), *array.shape))
    return lax.all_to_all(copies, axis, split_axis=0, concat_axis=0, tiled=True)


def of_everyone(array, axis):
    everything = sent_to_all(array, axis)
    return jnp.sum(everything, axis=0)


def block_pass(queries, keys_in, values_in, log_decay, block_len):
    num_blocks = queries.shape[0] // block_len

    def to_blocks(stacked):
        return stacked.reshape((num_blocks, block_len) + stacked.shape[1:])

    causal = jnp.tril(jnp.ones((block_len, block_len), dtype=bool))
    initial = (
        jnp.zeros((queries.shape[1], queries.shape[2], values_in.shape[2]), jnp.float32),
        jnp.zeros((queries.shape[1], queries.shape[2]), jnp.float32),
    )

    def advance(running, inputs):
        memory, offset = running
        block_q, block_k, block_v, block_g = inputs
        within = jnp.cumsum(block_g, axis=0)
        final_log = within[-1]
        scaled_q = block_q * jnp.exp(within)
        scaled_k = block_k * jnp.exp(-within)
        outside = jnp.einsum("ihd,hde->ihe", scaled_q, memory, precision=HIGHEST)
        scores = jnp.einsum("ihd,jhd->hij", scaled_q, scaled_k, precision=HIGHEST)
        scores = jnp.where(causal[None], scores, 0.0)
        inside = jnp.einsum("hij,jhe->ihe", scores, block_v, precision=HIGHEST)
        decayed_keys = scaled_k * jnp.exp(final_log)[None]
        memory = jnp.exp(final_log)[..., None] * memory + jnp.einsum(
            "jhd,jhe->hde", decayed_keys, block_v, precision=HIGHEST
        )
        carried_q = scaled_q * jnp.exp(offset)[None]
        return ((memory, offset + final_log), (outside + inside, carried_q))

    (memory, totals), (outputs, carried_q) = lax.scan(
        advance,
        initial,
        (to_blocks(queries), to_blocks(keys_in), to_blocks(values_in), to_blocks(log_decay)),
    )
    return (outputs.reshape(values_in.shape), carried_q.reshape(queries.shape), totals, memory)


def prepare(query, key_proj, value, decay, heads_here):
    row_count = query.shape[0]
    key_width = query.shape[1] // heads_here
    queries = query.astype(jnp.float32).reshape(row_count, heads_here, key_width) * key_width ** (
        -0.5
    )
    keys_in = key_proj.astype(jnp.float32).reshape(row_count, heads_here, key_width)
    values_in = value.astype(jnp.float32).reshape(
        row_count, heads_here, value.shape[1] // heads_here
    )
    log_decay = (
        jax.nn.log_sigmoid(decay.astype(jnp.float32)).reshape(row_count, heads_here, key_width)
        / DECAY_NORMALIZER
    )
    return (queries, keys_in, values_in, log_decay)


def finish(outputs, gate, head_gain):
    scale = lax.rsqrt(jnp.mean(jnp.square(outputs), axis=-1, keepdims=True) + EPS)
    gated = (
        outputs * scale * head_gain * jax.nn.silu(gate.astype(jnp.float32).reshape(outputs.shape))
    )
    return gated.reshape(outputs.shape[0], -1).astype(jnp.bfloat16)


def combine_states(earlier, later):
    return (
        earlier[0] + later[0],
        jnp.exp(later[0])[..., None] * earlier[1] + later[1],
        earlier[2] + later[2],
        jnp.exp(later[2])[..., None] * earlier[3] + later[3],
    )


def body(
    residual,
    query_wide,
    key_wide,
    value_wide,
    decay_wide,
    gate_wide,
    query_narrow,
    key_narrow,
    value_narrow,
    decay_narrow,
    gate_narrow,
    head_gain,
    out_wide,
    out_narrow,
    mlp_gain,
    up_weight,
    down_weight,
):
    heads_here = HEADS // lax.axis_size("tp")
    up_whole, down_whole = turned_gather((up_weight, down_weight), "sp", (0, 1))
    wq, wk, wv, wg = prepare(query_wide, key_wide, value_wide, decay_wide, heads_here)
    wide_out, wide_q, wide_total, wide_memory = block_pass(wq, wk, wv, wg, BLOCK)
    nq, nk, nv, ng = prepare(query_narrow, key_narrow, value_narrow, decay_narrow, heads_here)
    narrow_out, narrow_q, narrow_total, narrow_memory = block_pass(nq, nk, nv, ng, BLOCK)
    identity = (
        jnp.zeros_like(wide_total),
        jnp.zeros_like(wide_memory),
        jnp.zeros_like(narrow_total),
        jnp.zeros_like(narrow_memory),
    )
    incoming = entering(
        (wide_total, wide_memory, narrow_total, narrow_memory), "sp", combine_states, identity
    )
    wide_out = wide_out + jnp.einsum("ihd,hde->ihe", wide_q, incoming[1], precision=HIGHEST)
    narrow_out = narrow_out + jnp.einsum("ihd,hde->ihe", narrow_q, incoming[3], precision=HIGHEST)
    gated_wide = finish(wide_out, gate_wide, head_gain)
    gated_narrow = finish(narrow_out, gate_narrow, head_gain)
    head_terms = jnp.dot(gated_wide, out_wide, preferred_element_type=jnp.float32) + jnp.dot(
        gated_narrow, out_narrow, preferred_element_type=jnp.float32
    )
    tp_index = lax.axis_index("tp")
    col_count = residual.shape[1] // lax.axis_size("tp")
    full_width = residual.shape[1]
    residual_cols = lax.dynamic_slice_in_dim(residual, tp_index * col_count, col_count, 1)
    mixed_cols = sum_at_owner(head_terms.astype(jnp.bfloat16), "tp", 1)
    stream_cols = (residual_cols.astype(jnp.float32) + mixed_cols).astype(jnp.bfloat16)
    stream_f = stream_cols.astype(jnp.float32)
    squares = of_everyone(jnp.sum(jnp.square(stream_f), axis=1, keepdims=True), "tp")
    gain_cols = lax.dynamic_slice_in_dim(mlp_gain, tp_index * col_count, col_count, 0)
    normed_cols = (stream_f * lax.rsqrt(squares / full_width + EPS) * gain_cols).astype(
        jnp.bfloat16
    )
    normed = lax.all_gather(normed_cols, "tp", axis=1, tiled=True)
    before_activation = jnp.dot(normed, up_whole, preferred_element_type=jnp.float32)
    hidden = jnp.square(jax.nn.relu(before_activation)).astype(jnp.bfloat16)
    down_terms = jnp.dot(hidden, down_whole, preferred_element_type=jnp.float32)
    mlp_cols = sum_at_owner(down_terms.astype(jnp.bfloat16), "tp", 1)
    return (stream_cols.astype(jnp.float32) + mlp_cols).astype(jnp.bfloat16)


def solution(mesh):
    return jax.shard_map(
        body,
        mesh=mesh,
        in_specs=(
            P("sp", None),
            P("sp", "tp"),
            P("sp", "tp"),
            P("sp", "tp"),
            P("sp", "tp"),
            P("sp", "tp"),
            P("sp", "tp"),
            P("sp", "tp"),
            P("sp", "tp"),
            P("sp", "tp"),
            P("sp", "tp"),
            P(),
            P("tp", None),
            P("tp", None),
            P(),
            P("sp", "tp"),
            P("tp", "sp"),
        ),
        out_specs=P("sp", "tp"),
        check_vma=False,
    )
```

profile of v0, /device:TPU:0, one launch (start us, length us, event | category | flops | bytes accessed | tf_op | source)
XLA Modules:
  0.0 539.1 jit_solution(10759921777863404328)
XLA Ops:
  6.6 5.0 reshape.518
  13.8 1.7 broadcast.136.clone.1
  15.4 68.4 %while.51 = (s32[]{:T(128)}, f32[1,128,512]{2,1,0:T(8,128)S(1)}, f32[1,128]{1,0:T(1,128)S(1)}, f32[16,64,1,512]{3,1,2,0:T(8,128)}, f32[16,64,1,128]{3,1,2,0:T(8,...) while((s32[]{:T(128)}, f32[1,128,512]{2,1,0:T(8,128)S(1)}, ...), condition=%wide.region_5.6_spmd.clone, body=%wide.region_3.5_spmd.clone.sunk | while | flops 133005568 | bytes 2333321 | solution.py:98
  84.7 2.7 fusion.90
  87.3 3.3 reshape.501
  91.6 3.4 reshape.502
  95.0 4.9 reshape.516
  99.8 2.0 reshape.515
  101.9 1.6 broadcast.136.clone
  103.5 108.8 %while.50 = (s32[]{:T(128)}, f32[1,256,512]{2,1,0:T(8,128)S(1)}, f32[1,256]{1,0:T(1,128)S(1)}, f32[16,64,1,512]{3,1,2,0:T(8,128)}, f32[16,64,1,256]{3,1,2,0:T(8,...) while((s32[]{:T(128)}, f32[1,256,512]{2,1,0:T(8,128)S(1)}, ...), condition=%wide.region_2.3_spmd.clone, body=%wide.region_0.2_spmd.clone.sunk | while | flops 240787968 | bytes 3648133 | solution.py:98
  213.9 3.0 copy.32
  216.9 1.3 copy.33
  218.2 3.0 copy.34
  221.3 1.4 copy.35
  222.6 23.1 %all-gather.5 = bf16[32,1,128]{2,1,0:T(2,128)(2,1)S(1)} all-gather(bf16[1,1,128]{2,1,0:T(2,128)(2,1)S(1)} %convert_bitcast_fusion.1), channel_id=4, replica_groups=mesh['sp'=32,'tp'=4] {'sp'}, dimensions={0}, use_global_device_ids=true | all-gather | bytes 8448 | tf_op jit(solution)/shard_map/all_gather | solution.py:27
  245.7 23.8 %all-gather.4 = bf16[32,1,256]{2,1,0:T(2,128)(2,1)S(1)} all-gather(bf16[1,1,256]{2,1,0:T(2,128)(2,1)S(1)} %convert_bitcast_fusion), channel_id=2, replica_groups=mesh['sp'=32,'tp'=4] {'sp'}, dimensions={0}, use_global_device_ids=true | all-gather | bytes 16896 | tf_op jit(solution)/shard_map/all_gather | solution.py:27
  269.6 5.6 %multiply_reduce_fusion.1 = (f32[1024]{0:T(1024)S(1)}, f32[1024,1,512]{0,2,1:T(8,128)S(1)}) fusion(f32[1024,1,512]{0,2,1:T(8,128)} %copy.32, f32[1024,256]{1,0:T(8,128)} %bitcast.301, f32[1,256,512]{2,1,0:T(8,128)S(1)} %get-tuple-element.190), kind=kOutput, calls=%fused_computation.128 | convolution fusion | flops 1612184576 | bytes 5771264 | tf_op jit(solution)/shard_map/ihd,hde->ihe/dot_general | solution.py:174
  275.3 2.0 multiply_reduce_fusion
  277.4 2.8 fusion.87
  280.2 3.1 add_convert_fusion
  283.3 2.2 copy.90
  285.5 5.1 all-to-all-start
  290.7 48.5 %all-to-all-done = bf16[4,1024,512]{2,1,0:T(8,128)(2,1)} async-done(((bf16[4,1024,512]{2,1,0:T(8,128)(2,1)}), bf16[4,1024,512]{2,1,0:T(8,128)(2,1)}, u32[]{:S(2)}, u32[]{:S(2)}) %all-to-all-start) | async-done | bytes 4194336 | tf_op jit(solution)/shard_map/all_to_all | solution.py:54
  339.1 3.0 convert_reduce_fusion.1
  342.2 1.6 fusion.80
  344.4 3.3 all-to-all-start.1
  348.5 4.5 all-to-all-done.1
  354.4 111.0 %all-gather.11.cloned.1.call-done = bf16[1024,2048]{1,0:T(8,128)(2,1)} async-done(((bf16[1024,512]{1,0:T(8,128)(2,1)}), bf16[1024,2048]{1,0:T(8,128)(2,1)}) %all-gather.11.cloned.1.call-update) | async-done | bytes 4194320 | tf_op jit(solution)/shard_map/all_gather | solution.py:193
  465.4 8.1 %multiply_convert_fusion = bf16[1024,1024]{1,0:T(8,128)(2,1)S(1)} fusion(bf16[1024,2048]{1,0:T(8,128)(2,1)} %all-gather.11.cloned.1.call-done, bf16[2048,2048]{1,0:T(8,128)(2,1)} %all-gather.13.cloned.1.call-done), kind=kOutput, calls=%fused_computation.98 | convolution fusion | flops 4298113024 | bytes 10485760 | tf_op jit(solution)/shard_map/dot_general | solution.py:194
  473.5 4.8 fusion.63
  478.7 51.8 %all_to_all.15 = bf16[4,1024,512]{2,1,0:T(8,128)(2,1)S(1)} all-to-all(bf16[4,1024,512]{2,1,0:T(8,128)(2,1)S(1)} %bitcast.288), channel_id=1, replica_groups=mesh['sp'=32,'tp'=4] {'tp'}, dimensions={0} | all-to-all | bytes 8388608 | tf_op jit(solution)/shard_map/all_to_all | solution.py:54
  531.1 1.4 fusion.83
  (424 shorter events, 185.1 us)
Async XLA Ops:
  6.5 270.8 %copy-start = (bf16[512,2048]{1,0:T(8,128)(2,1)S(1)}, bf16[512,2048]{1,0:T(8,128)(2,1)}, u32[]{:S(2)}) copy-start(bf16[512,2048]{1,0:T(8,128)(2,1)} %param.35) | copy-start | bytes 6291460
  6.5 5.1 copy-start.10
  6.5 5.1 copy-start.11
  6.5 263.0 %all-gather.17.cloned.1.call-start = ((), (), s32[]{:S(2)}) async-start(), calls=%async_computation.6 | async-start | bytes 4325376 | tf_op jit(solution)/shard_map/all_gather | solution.py:27
  83.9 6.7 %copy-start.7 = (bf16[1024,256]{1,0:T(8,128)(2,1)S(1)}, bf16[1024,256]{1,0:T(8,128)(2,1)}, u32[]{:S(2)}) copy-start(bf16[1024,256]{1,0:T(8,128)(2,1)} %param.24) | copy-start | bytes 1572868
  84.6 184.9 %all-gather.15.cloned.1.call-start = ((), (), s32[]{:S(2)}) async-start(), calls=%async_computation.5 | async-start | bytes 8650752 | tf_op jit(solution)/shard_map/all_gather | solution.py:27
  91.6 8.2 %copy-start.8 = (bf16[1024,256]{1,0:T(8,128)(2,1)S(1)}, bf16[1024,256]{1,0:T(8,128)(2,1)}, u32[]{:S(2)}) copy-start(bf16[1024,256]{1,0:T(8,128)(2,1)} %param.25) | copy-start | bytes 1572868
  103.5 109.6 %copy-start.12 = (bf16[1024,64]{0,1:T(8,128)(2,1)S(1)}, bf16[1024,64]{0,1:T(8,128)(2,1)}, u32[]{:S(2)}) copy-start(bf16[1024,64]{0,1:T(8,128)(2,1)} %param.39) | copy-start | bytes 393220
  103.5 109.6 %copy-start.13 = (bf16[64,1024]{1,0:T(8,128)(2,1)S(1)}, bf16[64,1024]{1,0:T(8,128)(2,1)}, u32[]{:S(2)}) copy-start(bf16[64,1024]{1,0:T(8,128)(2,1)} %param.38) | copy-start | bytes 393220
  213.1 141.3 %all-gather.13.cloned.1.call-start = ((), (), s32[]{:S(2)}) async-start(), calls=%async_computation.4 | async-start | bytes 8650752 | tf_op jit(solution)/shard_map/all_gather | solution.py:16
  213.9 3.0 copy-start.3
  218.2 3.0 copy-start.4
  269.6 5.7 %copy-start.2 = (f32[1024,1,512]{0,2,1:T(8,128)S(1)}, f32[1024,1,512]{0,2,1:T(8,128)}, u32[]{:S(2)}) copy-start(f32[1024,1,512]{0,2,1:T(8,128)} %copy.34) | copy-start | bytes 6291460
  269.6 5.7 %copy-start.9 = (f32[16,64,1,128]{3,1,2,0:T(8,128)S(1)}, f32[16,64,1,128]{3,1,2,0:T(8,128)}, u32[]{:S(2)}) copy-start(f32[16,64,1,128]{3,1,2,0:T(8,128)} %get-tuple-element.194) | copy-start | bytes 1572868
  275.3 2.1 copy-start.6
  275.3 2.1 copy-start.16
  277.4 2.8 copy-start.5
  277.4 2.8 copy-start.15
  285.5 53.6 %all-to-all-start = ((bf16[4,1024,512]{2,1,0:T(8,128)(2,1)}), bf16[4,1024,512]{2,1,0:T(8,128)(2,1)}, u32[]{:S(2)}, u32[]{:S(2)}) async-start(bf16[4,1024,512]{2,1,0:T(8,128)(2,1)} %bitcast.287), calls=%async_computation | async-start | bytes 8388608 | tf_op jit(solution)/shard_map/all_to_all | solution.py:54
  344.4 8.6 %all-to-all-start.1 = ((f32[4,1024,1]{1,2,0:T(1,128)}), f32[4,1024,1]{1,2,0:T(1,128)S(1)}, u32[]{:S(2)}, u32[]{:S(2)}) async-start(f32[4,1024,1]{1,2,0:T(1,128)} %broadcast_in_dim.50), calls=%async_computation.1 | async-start | bytes 32768 | tf_op jit(solution)/shard_map/all_to_all | solution.py:60
  347.7 117.7 %all-gather.11.cloned.1.call-start = ((), (), s32[]{:S(2)}) async-start(), calls=%async_computation.3 | async-start | bytes 5242880 | tf_op jit(solution)/shard_map/all_gather | solution.py:193
  465.4 8.1 %copy-start.14 = (bf16[2048,2048]{1,0:T(8,128)(2,1)S(1)}, bf16[2048,2048]{1,0:T(8,128)(2,1)}, u32[]{:S(2)}) copy-start(bf16[2048,2048]{1,0:T(8,128)(2,1)} %all-gather.13.cloned.1.call-done) | copy-start | bytes 25165828
  530.4 2.1 copy-start.1
Sparse Core Ops, SparseCore 0:
  84.7 48.7 all-gather.16
  213.2 55.4 all-gather.14
  271.0 52.3 all-gather.12
  354.5 110.8 all-gather.10
where the time goes:
time: 545 us; the launch traced here: 539 us
  waiting for transfers between devices  164 us (30%)
  blocking collectives  98.6 us (18%)
  matrix products  91.9 us (17%)
  local copies, waits for them, and re-layouts  86.4 us (16%)
  other arithmetic  74.3 us (14%)
  between operations  13.5 us (2%)
  starting transfers between devices  8.53 us (2%)
    all_gather x1, waiting for transfers between devices, body(): normed = lax.all_gather(normed_cols, 'tp', axis=1, tiled=True)  111 us
    all_to_all x1, blocking collectives, sum_at_owner(): pieces = lax.all_to_all(split_up(array, dim, count), axis, 0, 0, tiled=True)  51.8 us
    all_to_all x1, waiting for transfers between devices, sum_at_owner(): pieces = lax.all_to_all(split_up(array, dim, count), axis, 0, 0, tiled=True)  48.5 us
    all_gather x2, blocking collectives, entering(): lax.all_gather(a.astype(kind), axis)  46.9 us
    dynamic_slice x48, local copies, waits for them, and re-layouts, block_pass(): lax.scan(advance, initial, (to_blocks(queries), to_blocks(keys_in), to_bl...  41.7 us
    dot_general x32, matrix products, advance(): outside = jnp.einsum('ihd,hde->ihe', scaled_q, memory, precision=HIGHEST)  22.1 us
    dot_general x32, matrix products, advance(): inside = jnp.einsum('hij,jhe->ihe', scores, block_v, precision=HIGHEST)  19.3 us
    dot_general x32, matrix products, advance(): jnp.einsum('jhd,jhe->hde', decayed_keys, block_v, precision=HIGHEST)  17.8 us
  transfers between devices with their start and end apart: 6, of which 3 were waited for; matrix products, arithmetic and copies ran while one was open for 30% of the time, Pallas kernels for 0%

commit v1 on v0

--- a/solution.py
+++ b/solution.py
@@ -190,7 +190,8 @@
     normed_cols = (stream_f * lax.rsqrt(squares / full_width + EPS) * gain_cols).astype(
         jnp.bfloat16
     )
-    normed = lax.all_gather(normed_cols, "tp", axis=1, tiled=True)
+    blocks = lax.all_gather(normed_cols, "tp")
+    normed = jnp.concatenate(blocks, axis=1)
     before_activation = jnp.dot(normed, up_whole, preferred_element_type=jnp.float32)
     hidden = jnp.square(jax.nn.relu(before_activation)).astype(jnp.bfloat16)
     down_terms = jnp.dot(hidden, down_whole, preferred_element_type=jnp.float32)

time: 545 us -> 605 us (1.11)
  waiting for transfers between devices: 164 us -> 213 us
  local copies, waits for them, and re-layouts: 86.4 us -> 94.9 us
    all_gather x1, waiting for transfers between devices: 0.02 us -> 49.1 us  [turned_gather(): lax.all_gather(both, axis, axis=0, tiled=True)]
    dot_general x1, matrix products: 4.8 us -> 14.4 us  [body(): down_terms = jnp.dot(hidden, down_whole, preferred_element_type=jnp.float32)]
    dot_general x1 -> x0, matrix products: 8.08 us -> none  [body(): jnp.dot(normed, up_whole, preferred_element_type=jnp.float32)]
    reshape x0 -> x1, local copies, waits for them, and re-layouts: none -> 6.28 us  [body(): normed = jnp.concatenate(blocks, axis=1)]
  transfers between devices with their start and end apart: 6 -> 6, of which waited for: 3 -> 5; matrix products, arithmetic and copies ran while one was open for 30% -> 24% of each run, Pallas kernels for 0% -> 0%
where the time goes in v1:
time: 605 us; the launch traced here: 599 us
  waiting for transfers between devices  213 us (35%)
  blocking collectives  100 us (17%)
  local copies, waits for them, and re-layouts  94.9 us (16%)
  matrix products  93.5 us (15%)
  other arithmetic  74.4 us (12%)
  between operations  13.5 us (2%)
  starting transfers between devices  8.45 us (1%)
    all_gather x1, waiting for transfers between devices, body(): blocks = lax.all_gather(normed_cols, 'tp')  110 us
    all_to_all x1, blocking collectives, sum_at_owner(): pieces = lax.all_to_all(split_up(array, dim, count), axis, 0, 0, tiled=True)  53.3 us
    all_gather x1, waiting for transfers between devices, turned_gather(): lax.all_gather(both, axis, axis=0, tiled=True)  49.1 us
    all_to_all x1, waiting for transfers between devices, sum_at_owner(): pieces = lax.all_to_all(split_up(array, dim, count), axis, 0, 0, tiled=True)  48.6 us
    all_gather x2, blocking collectives, entering(): lax.all_gather(a.astype(kind), axis)  46.8 us
    dynamic_slice x48, local copies, waits for them, and re-layouts, block_pass(): lax.scan(advance, initial, (to_blocks(queries), to_blocks(keys_in), to_bl...  41.7 us
    dot_general x32, matrix products, advance(): outside = jnp.einsum('ihd,hde->ihe', scaled_q, memory, precision=HIGHEST)  22.2 us
    dot_general x32, matrix products, advance(): inside = jnp.einsum('hij,jhe->ihe', scores, block_v, precision=HIGHEST)  19.4 us
  transfers between devices with their start and end apart: 6, of which 5 were waited for; matrix products, arithmetic and copies ran while one was open for 24% of the time, Pallas kernels for 0%

profile of v1, /device:TPU:0, one launch (start us, length us, event | category | flops | bytes accessed | tf_op | source)
XLA Modules:
  0.0 599.2 jit_solution(9157917397439504235)
XLA Ops:
  6.6 5.0 reshape.526
  13.8 1.6 broadcast.136.clone.1
  15.4 68.6 %while.51 = (s32[]{:T(128)}, f32[1,128,512]{2,1,0:T(8,128)S(1)}, f32[1,128]{1,0:T(1,128)S(1)}, f32[16,64,1,512]{3,1,2,0:T(8,128)}, f32[16,64,1,128]{3,1,2,0:T(8,...) while((s32[]{:T(128)}, f32[1,128,512]{2,1,0:T(8,128)S(1)}, ...), condition=%wide.region_5.6_spmd.clone, body=%wide.region_3.5_spmd.clone.sunk | while | flops 133005568 | bytes 2333321 | solution.py:98
  84.8 2.7 fusion.92
  87.5 3.3 reshape.507
  91.8 3.3 reshape.508
  95.1 4.9 reshape.524
  100.0 2.0 reshape.523
  102.0 1.6 broadcast.136.clone
  103.6 108.9 %while.50 = (s32[]{:T(128)}, f32[1,256,512]{2,1,0:T(8,128)S(1)}, f32[1,256]{1,0:T(1,128)S(1)}, f32[16,64,1,512]{3,1,2,0:T(8,128)}, f32[16,64,1,256]{3,1,2,0:T(8,...) while((s32[]{:T(128)}, f32[1,256,512]{2,1,0:T(8,128)S(1)}, ...), condition=%wide.region_2.3_spmd.clone, body=%wide.region_0.2_spmd.clone.sunk | while | flops 240787968 | bytes 3648133 | solution.py:98
  213.3 3.0 copy.39
  217.6 3.0 copy.41
  221.9 23.1 %all-gather.6 = bf16[32,1,128]{2,1,0:T(2,128)(2,1)S(1)} all-gather(bf16[1,1,128]{2,1,0:T(2,128)(2,1)S(1)} %convert_bitcast_fusion.1), channel_id=4, replica_groups=mesh['sp'=32,'tp'=4] {'sp'}, dimensions={0}, use_global_device_ids=true | all-gather | bytes 8448 | tf_op jit(solution)/shard_map/all_gather | solution.py:27
  245.0 23.7 %all-gather.5 = bf16[32,1,256]{2,1,0:T(2,128)(2,1)S(1)} all-gather(bf16[1,1,256]{2,1,0:T(2,128)(2,1)S(1)} %convert_bitcast_fusion), channel_id=2, replica_groups=mesh['sp'=32,'tp'=4] {'sp'}, dimensions={0}, use_global_device_ids=true | all-gather | bytes 16896 | tf_op jit(solution)/shard_map/all_gather | solution.py:27
  269.0 5.6 multiply_reduce_fusion.1
  274.7 2.0 multiply_reduce_fusion
  276.8 2.8 fusion.89
  279.6 3.1 add_convert_fusion
  282.6 2.3 copy.98
  285.0 5.1 all-to-all-start
  290.0 48.6 %all-to-all-done = bf16[4,1024,512]{2,1,0:T(8,128)(2,1)} async-done(((bf16[4,1024,512]{2,1,0:T(8,128)(2,1)}), bf16[4,1024,512]{2,1,0:T(8,128)(2,1)}, u32[]{:S(2)}, u32[]{:S(2)}) %all-to-all-start) | async-done | bytes 4194336 | tf_op jit(solution)/shard_map/all_to_all | solution.py:54
  338.6 3.0 convert_reduce_fusion.1
  341.7 1.6 fusion.80
  343.9 3.3 all-to-all-start.1
  348.0 4.6 all-to-all-done.1
  354.7 110.2 %all-gather.18.cloned.1.call-done = bf16[4096,512]{1,0:T(8,128)(2,1)} async-done(((bf16[1024,512]{1,0:T(8,128)(2,1)}), bf16[4096,512]{1,0:T(8,128)(2,1)}) %all-gather.18.cloned.1.call-update) | async-done | bytes 4194320 | tf_op jit(solution)/shard_map/all_gather | solution.py:193
  464.9 6.3 %copy.44 = bf16[1024,4,512]{0,2,1:T(8,128)(2,1)} copy(bf16[1024,4,512]{2,0,1:T(8,128)(2,1)} %bitcast.299) | data formatting | bytes 8388608 | tf_op jit(solution)/shard_map/reshape | solution.py:194
  471.2 49.1 %all-gather.12.cloned.1.call-done = bf16[2048,2048]{1,0:T(8,128)(2,1)} async-done(((bf16[64,2048]{1,0:T(8,128)(2,1)}), bf16[2048,2048]{1,0:T(8,128)(2,1)}) %all-gather.12.cloned.1.call-update) | async-done | bytes 8388624 | tf_op jit(solution)/shard_map/all_gather | solution.py:16
  520.3 14.4 %fusion.63 = bf16[1024,2048]{1,0:T(8,128)(2,1)} fusion(bf16[2048,2048]{1,0:T(8,128)(2,1)} %all-gather.12.cloned.1.call-done, bf16[1024,2048]{0,1:T(8,128)(2,1)} %bitcast.300), kind=kOutput, calls=%fused_computation.99 | convolution fusion | flops 8595177472 | bytes 16777216 | tf_op jit(solution)/shard_map/dot_general | solution.py:197
  534.7 2.6 copy.97
  537.3 53.3 %all_to_all.15 = bf16[4,1024,512]{2,1,0:T(8,128)(2,1)S(1)} all-to-all(bf16[4,1024,512]{2,1,0:T(8,128)(2,1)S(1)} %bitcast.291), channel_id=1, replica_groups=mesh['sp'=32,'tp'=4] {'tp'}, dimensions={0} | all-to-all | bytes 8388608 | tf_op jit(solution)/shard_map/all_to_all | solution.py:54
  591.2 1.4 fusion.83
  (422 shorter events, 187.8 us)
Async XLA Ops:
  6.5 270.2 %copy-start = (bf16[512,2048]{1,0:T(8,128)(2,1)S(1)}, bf16[512,2048]{1,0:T(8,128)(2,1)}, u32[]{:S(2)}) copy-start(bf16[512,2048]{1,0:T(8,128)(2,1)} %param.35) | copy-start | bytes 6291460
  6.5 5.1 copy-start.10
  6.5 5.1 copy-start.11
  6.5 262.1 %all-gather.16.cloned.1.call-start = ((), (), s32[]{:S(2)}) async-start(), calls=%async_computation.5 | async-start | bytes 4325376 | tf_op jit(solution)/shard_map/all_gather | solution.py:27
  84.0 6.8 %copy-start.7 = (bf16[1024,256]{1,0:T(8,128)(2,1)S(1)}, bf16[1024,256]{1,0:T(8,128)(2,1)}, u32[]{:S(2)}) copy-start(bf16[1024,256]{1,0:T(8,128)(2,1)} %param.24) | copy-start | bytes 1572868
  84.7 184.2 %all-gather.14.cloned.1.call-start = ((), (), s32[]{:S(2)}) async-start(), calls=%async_computation.4 | async-start | bytes 8650752 | tf_op jit(solution)/shard_map/all_gather | solution.py:27
  91.8 8.2 %copy-start.8 = (bf16[1024,256]{1,0:T(8,128)(2,1)S(1)}, bf16[1024,256]{1,0:T(8,128)(2,1)}, u32[]{:S(2)}) copy-start(bf16[1024,256]{1,0:T(8,128)(2,1)} %param.25) | copy-start | bytes 1572868
  213.3 3.0 copy-start.3
  217.6 3.0 copy-start.4
  269.0 5.7 copy-start.2
  269.0 5.7 copy-start.9
  274.7 2.1 copy-start.6
  274.7 2.1 copy-start.15
  276.8 2.8 copy-start.5
  276.8 2.8 copy-start.14
  285.0 53.7 %all-to-all-start = ((bf16[4,1024,512]{2,1,0:T(8,128)(2,1)}), bf16[4,1024,512]{2,1,0:T(8,128)(2,1)}, u32[]{:S(2)}, u32[]{:S(2)}) async-start(bf16[4,1024,512]{2,1,0:T(8,128)(2,1)} %bitcast.290), calls=%async_computation | async-start | bytes 8388608 | tf_op jit(solution)/shard_map/all_to_all | solution.py:54
  343.3 10.7 %copy-start.12 = (bf16[1024,64]{0,1:T(8,128)(2,1)S(1)}, bf16[1024,64]{0,1:T(8,128)(2,1)}, u32[]{:S(2)}) copy-start(bf16[1024,64]{0,1:T(8,128)(2,1)} %param.39) | copy-start | bytes 393220
  343.3 10.7 %copy-start.13 = (bf16[64,1024]{1,0:T(8,128)(2,1)S(1)}, bf16[64,1024]{1,0:T(8,128)(2,1)}, u32[]{:S(2)}) copy-start(bf16[64,1024]{1,0:T(8,128)(2,1)} %param.38) | copy-start | bytes 393220
  343.9 8.6 %all-to-all-start.1 = ((f32[4,1024,1]{1,2,0:T(1,128)}), f32[4,1024,1]{1,2,0:T(1,128)S(1)}, u32[]{:S(2)}, u32[]{:S(2)}) async-start(f32[4,1024,1]{1,2,0:T(1,128)} %broadcast_in_dim.50), calls=%async_computation.1 | async-start | bytes 32768 | tf_op jit(solution)/shard_map/all_to_all | solution.py:60
  347.2 117.8 %all-gather.18.cloned.1.call-start = ((), (), s32[]{:S(2)}) async-start(), calls=%async_computation.6 | async-start | bytes 5242880 | tf_op jit(solution)/shard_map/all_gather | solution.py:193
  353.9 166.4 %all-gather.12.cloned.1.call-start = ((), (), s32[]{:S(2)}) async-start(), calls=%async_computation.3 | async-start | bytes 8650752 | tf_op jit(solution)/shard_map/all_gather | solution.py:16
  590.6 2.1 copy-start.1
Sparse Core Ops, SparseCore 0:
  84.8 48.6 all-gather.15
  213.4 55.4 all-gather.13
  354.0 110.8 all-gather.17
  467.1 53.2 all-gather.11
